TPU v7x, 32 devices: a whole 2x2x4 slice. The times are simulated.
32 devices in a mesh: ep: 8 (over z, core), tp: 4 (over y, x).
Axes of the slice: x: 2, y: 2, z: 4, core: 2. Of those that a mesh axis runs over, the one named last changes fastest.
Arguments:
- tokens: bfloat16 [1024, 4096], P('ep', 'tp'), may hold values from -6 to 6
- out_grad: bfloat16 [1024, 4096], P('ep', 'tp'), may hold values from -1.5 to 1.5
- routes: int32 [1024, 2], P('ep'), may hold values from 0 to 7, all different within a row; in each aligned block of 128 rows (0 to 127, 128 to 255, ...) at most 40 rows name the same one
- route_weights: float32 [1024, 2], P('ep'), may hold values from 0.2 to 1.2
- gate_proj: bfloat16 [8, 1024, 4096], P('ep', 'tp'), may hold values from -0.09375 to 0.09375
- up_proj: bfloat16 [8, 1024, 4096], P('ep', 'tp'), may hold values from -0.09375 to 0.09375
- down_proj: bfloat16 [8, 1024, 4096], P('ep', 'tp'), may hold values from -0.1875 to 0.1875
- shared_hidden: bfloat16 [1024, 1024], P('ep'), may hold values from -6 to 6
Outputs:
- token_grad: bfloat16 [1024, 4096], P('ep', 'tp')
- weight_grad: float32 [1024, 2], P('ep')
- gate_grad: bfloat16 [8, 1024, 4096], P('ep', 'tp')
- up_grad: bfloat16 [8, 1024, 4096], P('ep', 'tp')
- down_grad: bfloat16 [8, 1024, 4096], P('ep', 'tp')
- shared_grad: float32 [1024, 4096], P('ep', 'tp')
Inputs may be any that keep to these rules, and one draw needn't show every extreme that they name: Within each block of 128 consecutive tokens, no expert is named by more than 40 routes, and in some blocks one expert is named by exactly 40. The 2 experts of one token differ.
All inputs are finite; a program needn't handle non-finite values.
Results may differ from a plain program's by a relative error of at most 0.0065.
Values may be sent and summed in bfloat16 or wider, within the bound.
A program may use at most 64 MiB of HBM per device.

v0:
```python
import jax
import jax.numpy as jnp
from jax import lax
from jax.sharding import PartitionSpec as P


def slot_tables(routes, num_experts, capacity):
    tok_rows, per_token = routes.shape
    route_count = tok_rows * per_token
    flat_routes = routes.reshape(-1)
    expert_ids = lax.broadcasted_iota(jnp.int32, (route_count, num_experts), 1)
    onehot = (flat_routes[:, None] == expert_ids).astype(jnp.int32)
    slot_rank = jnp.sum((jnp.cumsum(onehot, axis=0) - 1) * onehot, axis=1)
    slot_of_route = flat_routes * capacity + slot_rank
    slot_ids = lax.broadcasted_iota(jnp.int32, (num_experts * capacity, route_count), 0)
    route_ids = lax.broadcasted_iota(jnp.int32, (num_experts * capacity, route_count), 1)
    matches = slot_ids == slot_of_route[None, :]
    route_of_slot = jnp.sum(jnp.where(matches, route_ids, 0), axis=1)
    filled = jnp.any(matches, axis=1)
    return (slot_of_route, route_of_slot, filled)


def local(tokens, out_grad, routes, route_weights, gate_proj, up_proj, down_proj, shared_hidden):
    ep_count = lax.axis_size("ep")
    tp_count = lax.axis_size("tp")
    local_experts = gate_proj.shape[0]
    num_experts = local_experts * ep_count
    tok_rows, per_token = routes.shape
    capacity = max(2, 5 * tok_rows * per_token // (4 * num_experts))
    slot_of_route, route_of_slot, filled = slot_tables(routes, num_experts, capacity)
    token_of_slot = route_of_slot // per_token
    zero_value = jnp.zeros((), jnp.bfloat16)
    slot_weight = jnp.where(filled, route_weights.reshape(-1)[route_of_slot], 0.0)
    slot_weight = slot_weight.astype(jnp.bfloat16).reshape(ep_count, local_experts, capacity)
    layout = (ep_count, local_experts, capacity, -1)
    sent_tokens = jnp.where(filled[:, None], tokens[token_of_slot], zero_value).reshape(layout)
    sent_grads = jnp.where(filled[:, None], out_grad[token_of_slot], zero_value).reshape(layout)
    part_tokens, part_grads, weights_in = (
        lax.all_to_all(sent_tokens, "ep", split_axis=0, concat_axis=2, tiled=True),
        lax.all_to_all(sent_grads, "ep", split_axis=0, concat_axis=2, tiled=True),
        lax.all_to_all(slot_weight, "ep", split_axis=0, concat_axis=2, tiled=True),
    )
    rows_in, grads_in = (
        lax.all_gather(part_tokens, "tp", axis=3, tiled=True),
        lax.all_gather(part_grads, "tp", axis=3, tiled=True),
    )
    rows_in = rows_in[0]
    grads_in = grads_in[0]
    slot_scale = weights_in[0].astype(jnp.float32)
    pre_gate = jnp.einsum("lrd,lfd->lrf", rows_in, gate_proj, preferred_element_type=jnp.float32)
    pre_up = jnp.einsum("lrd,lfd->lrf", rows_in, up_proj, preferred_element_type=jnp.float32)
    squash = jax.nn.sigmoid(pre_gate)
    activated = pre_gate * squash
    hidden = (activated * pre_up).astype(jnp.bfloat16)
    back_grad = jnp.einsum("lrd,lfd->lrf", grads_in, down_proj, preferred_element_type=jnp.float32)
    partial_products = jnp.sum(hidden.astype(jnp.float32) * back_grad, axis=2)
    hidden_grad = slot_scale[:, :, None] * back_grad
    scaled_hidden = (slot_scale[:, :, None] * hidden.astype(jnp.float32)).astype(jnp.bfloat16)
    gate_delta = (hidden_grad * pre_up * squash * (1.0 + pre_gate * (1.0 - squash))).astype(
        jnp.bfloat16
    )
    up_delta = (hidden_grad * activated).astype(jnp.bfloat16)
    gate_grad = jnp.einsum(
        "lrf,lrd->lfd", gate_delta, rows_in, preferred_element_type=jnp.float32
    ).astype(jnp.bfloat16)
    up_grad = jnp.einsum(
        "lrf,lrd->lfd", up_delta, rows_in, preferred_element_type=jnp.float32
    ).astype(jnp.bfloat16)
    down_grad = jnp.einsum(
        "lrf,lrd->lfd", scaled_hidden, grads_in, preferred_element_type=jnp.float32
    ).astype(jnp.bfloat16)
    partial_rows = jnp.einsum(
        "lrf,lfd->lrd", gate_delta, gate_proj, preferred_element_type=jnp.float32
    )
    partial_rows = partial_rows + jnp.einsum(
        "lrf,lfd->lrd", up_delta, up_proj, preferred_element_type=jnp.float32
    )
    partial_rows = partial_rows.astype(jnp.bfloat16)
    gathered = lax.all_to_all(partial_rows, "tp", split_axis=2, concat_axis=0, tiled=True)
    gathered = gathered.reshape((tp_count,) + partial_rows.shape[:2] + (-1,))
    summed = jnp.sum(gathered, axis=0, dtype=jnp.float32)
    products = lax.psum(partial_products, "tp")
    slot_rows, slot_products = (
        lax.all_to_all(summed[None], "ep", split_axis=2, concat_axis=0, tiled=True),
        lax.all_to_all(products[None], "ep", split_axis=2, concat_axis=0, tiled=True),
    )
    feature_width = slot_rows.shape[-1]
    slot_rows = slot_rows.reshape(num_experts * capacity, feature_width)
    route_rows = slot_rows[slot_of_route].reshape(tok_rows, per_token, feature_width)
    token_grad = jnp.sum(route_rows, axis=1).astype(jnp.bfloat16)
    weight_grad = slot_products.reshape(-1)[slot_of_route].reshape(tok_rows, per_token)
    shared_grad = lax.psum_scatter(
        lax.dot_general(
            shared_hidden, out_grad, (((0,), (0,)), ((), ())), preferred_element_type=jnp.float32
        ),
        "ep",
        scatter_dimension=0,
        tiled=True,
    )
    return (token_grad, weight_grad, gate_grad, up_grad, down_grad, shared_grad)


def solution(mesh):
    return jax.shard_map(
        local,
        mesh=mesh,
        in_specs=(
            P("ep", "tp"),
            P("ep", "tp"),
            P("ep", None),
            P("ep", None),
            P("ep", "tp", None),
            P("ep", "tp", None),
            P("ep", "tp", None),
            P("ep", None),
        ),
        out_specs=(
            P("ep", "tp"),
            P("ep", None),
            P("ep", "tp", None),
            P("ep", "tp", None),
            P("ep", "tp", None),
            P("ep", "tp"),
        ),
        check_vma=False,
    )
```

profile of v0, /device:TPU:0, one launch (start us, length us, event | category | flops | bytes accessed | tf_op | source)
XLA Modules:
  0.0 350.5 jit_solution(12991959504227618092)
XLA Ops:
  10.6 2.6 gather_fusion.1
  17.5 24.5 %all_to_all.60 = bf16[8,1,40,1024]{3,2,1,0:T(8,128)(2,1)} all-to-all(bf16[8,1,40,1024]{3,2,1,0:T(8,128)(2,1)S(1)} %get-tuple-element.43), channel_id=1, replica_groups=mesh['ep'=8,'tp'=4] {'ep'}, dimensions={0} | all-to-all | bytes 1310720 | tf_op jit(solution)/shard_map/all_to_all | solution.py:39
  42.1 21.2 %all_to_all.61 = bf16[8,1,40,1024]{3,2,1,0:T(8,128)(2,1)} all-to-all(bf16[8,1,40,1024]{3,2,1,0:T(8,128)(2,1)S(1)} %get-tuple-element.42), channel_id=1, replica_groups=mesh['ep'=8,'tp'=4] {'ep'}, dimensions={0} | all-to-all | bytes 1310720 | tf_op jit(solution)/shard_map/all_to_all | solution.py:40
  63.4 2.8 fusion.30
  69.6 8.1 %all_to_all.62 = bf16[8,1,40]{2,1,0:T(2,128)(2,1)S(1)} all-to-all(bf16[8,1,40]{2,1,0:T(2,128)(2,1)S(1)} %convert_element_type.110), channel_id=1, replica_groups=mesh['ep'=8,'tp'=4] {'ep'}, dimensions={0} | all-to-all | bytes 1280 | tf_op jit(solution)/shard_map/all_to_all | solution.py:41
  77.8 2.8 all-gather.5.cloned.1.call-done
  80.6 2.8 fusion.7
  84.8 37.3 %all-gather.3.cloned.1.call-done = bf16[1,1,320,4096]{3,2,1,0:T(8,128)(2,1)} async-done(((bf16[1,1,320,1024]{3,2,1,0:T(8,128)(2,1)}), bf16[1,1,320,4096]{3,2,1,0:T(8,128)(2,1)}) %all-gather.3.cloned.1.call-update) | async-done | bytes 2621456 | tf_op jit(solution)/shard_map/all_gather | solution.py:45
  122.0 3.4 fusion.20
  129.4 14.3 %copy.56 = bf16[1,320,4096]{1,0,2:T(2,128)(2,1)} copy(bf16[1,320,4096]{2,1,0:T(8,128)(2,1)} %fusion.1) | data formatting | bytes 5242880 | tf_op jit(solution)/shard_map/convert_element_type | solution.py:78
  144.3 68.8 %reduce.16 = bf16[4096,320]{1,0:T(8,128)(2,1)} reduce(bf16[4096,1,320]{2,1,0:T(2,128)(2,1)} %bitcast.67, bf16[]{:T(256)} %broadcast.230), dimensions={1}, to_apply=%bitcast.53.reduce_sub_computation | reduce | bytes 5242882
  213.0 6.1 %reshape.388 = bf16[4,2,163840]{2,1,0:T(2,128)(2,1)} reshape(bf16[4096,320]{1,0:T(8,128)(2,1)} %reduce.16) | data formatting | bytes 5242880
  219.2 4.6 %all-to-all-start.3 = ((bf16[4,2,163840]{2,1,0:T(2,128)(2,1)}), bf16[4,2,163840]{2,1,0:T(2,128)(2,1)}, u32[]{:S(2)}, u32[]{:S(2)}) async-start(bf16[4,2,163840]{2,1,0:T(2,128)(2,1)} %reshape.388), calls=%async_computation.3 | async-start | bytes 5242880 | tf_op jit(solution)/shard_map/all_to_all | solution.py:79
  223.8 33.7 %psum.7 = f32[1,1,320]{2,1,0:T(1,128)S(1)} all-reduce(f32[1,1,320]{2,1,0:T(1,128)S(1)} %broadcast_in_dim.48), channel_id=1, replica_groups=mesh['ep'=8,'tp'=4] {'tp'}, use_global_device_ids=true, to_apply=%region_8.9 | all-reduce | flops 320 | bytes 2560 | tf_op jit(solution)/shard_map/psum | solution.py:82
  258.3 4.6 %all-to-all-start.5 = ((f32[1,1,320]{1,0,2:T(1,128)}), f32[1,1,320]{1,0,2:T(1,128)S(1)}, u32[]{:S(2)}, u32[]{:S(2)}) async-start(f32[1,1,320]{1,0,2:T(1,128)} %copy.59), calls=%async_computation.5 | async-start | bytes 327680 | tf_op jit(solution)/shard_map/all_to_all | solution.py:85
  262.9 7.6 %reshape.389 = bf16[4096,1,320]{2,1,0:T(2,128)(2,1)} reshape(bf16[4,2,163840]{2,1,0:T(2,128)(2,1)} %all-to-all-done.3) | data formatting | bytes 5242880
  270.5 14.0 %copy.57 = bf16[1,320,4096]{2,1,0:T(8,128)(2,1)} copy(bf16[1,320,4096]{1,0,2:T(2,128)(2,1)} %bitcast.68) | data formatting | bytes 5242880 | tf_op jit(solution)/shard_map/all_to_all | solution.py:79
  284.5 7.3 %reshape.336 = f32[320,4,1024]{2,1,0:T(4,128)} reshape(bf16[1,320,4096]{2,1,0:T(8,128)(2,1)} %copy.57) | data formatting | bytes 7864320 | tf_op jit(solution)/shard_map/convert_element_type | solution.py:81
  291.8 5.7 %reduce_sum.54 = f32[320,1024]{1,0:T(8,128)S(1)} reduce(f32[320,4,1024]{2,1,0:T(4,128)} %reshape.336, f32[]{:T(128)} %constant.33.clone.1), dimensions={1}, to_apply=%region_5.6 | reduce | flops 983040 | bytes 6553604 | tf_op jit(solution)/shard_map/reduce_sum | solution.py:81
  299.5 5.1 %all-to-all-start.4 = ((f32[1,1,320,1024]{3,1,0,2:T(1,128)}), f32[1,1,320,1024]{3,1,0,2:T(1,128)S(1)}, u32[]{:S(2)}, u32[]{:S(2)}) async-start(f32[1,1,320,1024]{3,1,0,2:T(1,128)} %broadcast_in_dim.47), calls=%async_computation.4 | async-start | bytes 2621440 | tf_op jit(solution)/shard_map/all_to_all | solution.py:84
  304.9 4.3 %fusion.2 = bf16[1,256,4096]{2,1,0:T(8,128)(2,1)} fusion(bf16[320,256]{1,0:T(8,128)(2,1)S(1)} %get-tuple-element.40, bf16[1,1,320,4096]{3,2,1,0:T(8,128)(2,1)} %all-gather.5.cloned.1.call-done), kind=kOutput, calls=%fused_computation.11 | convolution fusion | flops 672137216 | bytes 4882432 | tf_op jit(solution)/shard_map/lrf,lrd->lfd/dot_general | solution.py:63
  309.3 4.5 %fusion.3 = bf16[1,256,4096]{2,1,0:T(8,128)(2,1)} fusion(bf16[320,256]{1,0:T(8,128)(2,1)S(1)} %get-tuple-element.41, bf16[1,1,320,4096]{3,2,1,0:T(8,128)(2,1)} %all-gather.5.cloned.1.call-done), kind=kOutput, calls=%fused_computation.12 | convolution fusion | flops 672137216 | bytes 4882432 | tf_op jit(solution)/shard_map/lrf,lrd->lfd/dot_general | solution.py:66
  313.7 2.7 fusion.4
  320.2 16.6 %all-to-all-done.4 = f32[1,1,320,1024]{3,1,0,2:T(1,128)S(1)} async-done(((f32[1,1,320,1024]{3,1,0,2:T(1,128)}), f32[1,1,320,1024]{3,1,0,2:T(1,128)S(1)}, u32[]{:S(2)}, u32[]{:S(2)}) %all-to-all-start.4) | async-done | bytes 1310752 | tf_op jit(solution)/shard_map/all_to_all | solution.py:84
  (75 shorter events, 29.2 us)
Async XLA Ops:
  8.0 72.6 %copy-start = (bf16[1,256,4096]{2,1,0:T(8,128)(2,1)S(1)}, bf16[1,256,4096]{2,1,0:T(8,128)(2,1)}, u32[]{:S(2)}) copy-start(bf16[1,256,4096]{2,1,0:T(8,128)(2,1)} %param.12) | copy-start | bytes 6291460
  8.0 2.6 copy-start.2
  8.0 72.6 %all-gather.5.cloned.1.call-start = ((), (), s32[]{:S(2)}) async-start(), calls=%async_computation.8 | async-start | bytes 3276800 | tf_op jit(solution)/shard_map/all_gather | solution.py:44
  10.6 2.7 copy-start.3
  17.5 45.9 %copy-start.8 = (bf16[128,1024]{1,0:T(8,128)(2,1)S(1)}, bf16[128,1024]{1,0:T(8,128)(2,1)}, u32[]{:S(2)}) copy-start(bf16[128,1024]{1,0:T(8,128)(2,1)} %param.15) | copy-start | bytes 786436
  42.0 80.0 %all-gather.3.cloned.1.call-start = ((), (), s32[]{:S(2)}) async-start(), calls=%async_computation.7 | async-start | bytes 3276800 | tf_op jit(solution)/shard_map/all_gather | solution.py:45
  63.3 279.7 %reduce-scatter.2.cloned.1.call-start = ((), (), s32[]{:S(2)}) async-start(), calls=%async_computation.9 | async-start | bytes 4718592 | tf_op jit(solution)/shard_map/reduce_scatter | solution.py:92
  66.2 0.7 copy-start.10
  80.6 2.8 copy-start.4
  80.6 3.2 copy-start.6
  125.4 1.6 copy-start.7
  219.2 39.1 %all-to-all-start.3 = ((bf16[4,2,163840]{2,1,0:T(2,128)(2,1)}), bf16[4,2,163840]{2,1,0:T(2,128)(2,1)}, u32[]{:S(2)}, u32[]{:S(2)}) async-start(bf16[4,2,163840]{2,1,0:T(2,128)(2,1)} %reshape.388), calls=%async_computation.3 | async-start | bytes 5242880 | tf_op jit(solution)/shard_map/all_to_all | solution.py:79
  258.3 41.2 %all-to-all-start.5 = ((f32[1,1,320]{1,0,2:T(1,128)}), f32[1,1,320]{1,0,2:T(1,128)S(1)}, u32[]{:S(2)}, u32[]{:S(2)}) async-start(f32[1,1,320]{1,0,2:T(1,128)} %copy.59), calls=%async_computation.5 | async-start | bytes 327680 | tf_op jit(solution)/shard_map/all_to_all | solution.py:85
  297.5 7.1 %copy-start.9 = (s32[128,2]{0,1:T(2,128)S(1)}, s32[128,2]{0,1:T(2,128)}, u32[]{:S(2)}) copy-start(s32[128,2]{0,1:T(2,128)} %param.10) | copy-start | bytes 3076
  299.5 37.3 %all-to-all-start.4 = ((f32[1,1,320,1024]{3,1,0,2:T(1,128)}), f32[1,1,320,1024]{3,1,0,2:T(1,128)S(1)}, u32[]{:S(2)}, u32[]{:S(2)}) async-start(f32[1,1,320,1024]{3,1,0,2:T(1,128)} %broadcast_in_dim.47), calls=%async_computation.4 | async-start | bytes 2621440 | tf_op jit(solution)/shard_map/all_to_all | solution.py:84
  309.3 4.5 %copy-start.5 = (bf16[1,1,320,4096]{3,2,1,0:T(8,128)(2,1)S(1)}, bf16[1,1,320,4096]{3,2,1,0:T(8,128)(2,1)}, u32[]{:S(2)}) copy-start(bf16[1,1,320,4096]{3,2,1,0:T(8,128)(2,1)} %all-gather.3.cloned.1.call-done) | copy-start | bytes 7864324
  337.1 6.0 %copy-start.1 = (bf16[1,256,4096]{2,1,0:T(8,128)(2,1)S(1)}, bf16[1,256,4096]{2,1,0:T(8,128)(2,1)}, u32[]{:S(2)}) copy-start(bf16[1,256,4096]{2,1,0:T(8,128)(2,1)} %param.12) | copy-start | bytes 6291460
Sparse Core Ops, SparseCore 0:
  42.1 38.4 all-gather.4
  82.5 39.4 all-gather.2
Sparse Core Ops, SparseCore 1:
  66.7 48.8 reduce-scatter.1
where the time goes:
time: 352 us; the launch traced here: 350 us
  blocking collectives  87.6 us (25%)
  other arithmetic  80.1 us (23%)
  local copies, waits for them, and re-layouts  71.3 us (20%)
  waiting for transfers between devices  56.7 us (16%)
  matrix products  24.6 us (7%)
  between operations  15.7 us (4%)
  starting transfers between devices  14.4 us (4%)
    unnamed x1, other arithmetic  68.8 us
    all_gather x1, waiting for transfers between devices, local(): lax.all_gather(part_grads, 'tp', axis=3, tiled=True)  37.3 us
    psum x1, blocking collectives, local(): products = lax.psum(partial_products, 'tp')  33.7 us
    all_to_all x1, blocking collectives, local(): lax.all_to_all(sent_tokens, 'ep', split_axis=0, concat_axis=2, tiled=True)  24.5 us
    all_to_all x1, blocking collectives, local(): lax.all_to_all(sent_grads, 'ep', split_axis=0, concat_axis=2, tiled=True)  21.2 us
    unnamed x29, local copies, waits for them, and re-layouts  18.1 us
    all_to_all x1, waiting for transfers between devices, local(): lax.all_to_all(summed[None], 'ep', split_axis=2, concat_axis=0, tiled=True)  16.6 us
    convert_element_type x1, local copies, waits for them, and re-layouts, local(): partial_rows = partial_rows.astype(jnp.bfloat16)  14.3 us
  transfers between devices with their start and end apart: 6, of which 3 were waited for; matrix products, arithmetic and copies ran while one was open for 47% of the time, Pallas kernels for 0%

commit v1 on v0

--- a/solution.py
+++ b/solution.py
@@ -79,7 +79,9 @@
     gathered = lax.all_to_all(partial_rows, "tp", split_axis=2, concat_axis=0, tiled=True)
     gathered = gathered.reshape((tp_count,) + partial_rows.shape[:2] + (-1,))
     summed = jnp.sum(gathered, axis=0, dtype=jnp.float32)
-    products = lax.psum(partial_products, "tp")
+    products = partial_products
+    for hop in (1, 2):
+        products = products + lax.ppermute(products, "tp", [(dev, dev ^ hop) for dev in range(4)])
     slot_rows, slot_products = (
         lax.all_to_all(summed[None], "ep", split_axis=2, concat_axis=0, tiled=True),
         lax.all_to_all(products[None], "ep", split_axis=2, concat_axis=0, tiled=True),

time: 352 us -> 353 us (level)
  blocking collectives: 87.6 us -> 53.9 us
  waiting for transfers between devices: 56.7 us -> 87.5 us
    psum x1 -> x0, blocking collectives: 33.7 us -> none  [local(): products = lax.psum(partial_products, 'tp')]
    ppermute x0 -> x2, waiting for transfers between devices: none -> 30.8 us  [local(): lax.ppermute(products, 'tp', [(dev, dev ^ hop) for dev in range(4)])]
  transfers between devices with their start and end apart: 6 -> 8, of which waited for: 3 -> 5; matrix products, arithmetic and copies ran while one was open for 47% -> 47% of each run, Pallas kernels for 0% -> 0%
where the time goes in v1:
time: 353 us; the launch traced here: 351 us
  waiting for transfers between devices  87.5 us (25%)
  other arithmetic  80.1 us (23%)
  local copies, waits for them, and re-layouts  71.3 us (20%)
  blocking collectives  53.9 us (15%)
  matrix products  24.6 us (7%)
  starting transfers between devices  17.8 us (5%)
  between operations  15.7 us (4%)
    unnamed x1, other arithmetic  68.8 us
    all_gather x1, waiting for transfers between devices, local(): lax.all_gather(part_grads, 'tp', axis=3, tiled=True)  37.3 us
    ppermute x2, waiting for transfers between devices, local(): lax.ppermute(products, 'tp', [(dev, dev ^ hop) for dev in range(4)])  30.8 us
    all_to_all x1, blocking collectives, local(): lax.all_to_all(sent_tokens, 'ep', split_axis=0, concat_axis=2, tiled=True)  24.5 us
    all_to_all x1, blocking collectives, local(): lax.all_to_all(sent_grads, 'ep', split_axis=0, concat_axis=2, tiled=True)  21.2 us
    unnamed x29, local copies, waits for them, and re-layouts  18.1 us
    all_to_all x1, waiting for transfers between devices, local(): lax.all_to_all(summed[None], 'ep', split_axis=2, concat_axis=0, tiled=True)  16.6 us
    convert_element_type x1, local copies, waits for them, and re-layouts, local(): partial_rows = partial_rows.astype(jnp.bfloat16)  14.3 us
  transfers between devices with their start and end apart: 8, of which 5 were waited for; matrix products, arithmetic and copies ran while one was open for 47% of the time, Pallas kernels for 0%

profile of v1, /device:TPU:0, one launch (start us, length us, event | category | flops | bytes accessed | tf_op | source)
XLA Modules:
  0.0 351.0 jit_solution(6714992095780923295)
XLA Ops:
  10.6 2.6 gather_fusion.1
  17.5 24.5 %all_to_all.60 = bf16[8,1,40,1024]{3,2,1,0:T(8,128)(2,1)} all-to-all(bf16[8,1,40,1024]{3,2,1,0:T(8,128)(2,1)S(1)} %get-tuple-element.43), channel_id=1, replica_groups=mesh['ep'=8,'tp'=4] {'ep'}, dimensions={0} | all-to-all | bytes 1310720 | tf_op jit(solution)/shard_map/all_to_all | solution.py:39
  42.1 21.2 %all_to_all.61 = bf16[8,1,40,1024]{3,2,1,0:T(8,128)(2,1)} all-to-all(bf16[8,1,40,1024]{3,2,1,0:T(8,128)(2,1)S(1)} %get-tuple-element.42), channel_id=1, replica_groups=mesh['ep'=8,'tp'=4] {'ep'}, dimensions={0} | all-to-all | bytes 1310720 | tf_op jit(solution)/shard_map/all_to_all | solution.py:40
  63.4 2.8 fusion.30
  69.6 8.1 %all_to_all.62 = bf16[8,1,40]{2,1,0:T(2,128)(2,1)S(1)} all-to-all(bf16[8,1,40]{2,1,0:T(2,128)(2,1)S(1)} %convert_element_type.110), channel_id=1, replica_groups=mesh['ep'=8,'tp'=4] {'ep'}, dimensions={0} | all-to-all | bytes 1280 | tf_op jit(solution)/shard_map/all_to_all | solution.py:41
  77.8 2.8 all-gather.5.cloned.1.call-done
  80.6 2.8 fusion.7
  84.8 37.3 %all-gather.3.cloned.1.call-done = bf16[1,1,320,4096]{3,2,1,0:T(8,128)(2,1)} async-done(((bf16[1,1,320,1024]{3,2,1,0:T(8,128)(2,1)}), bf16[1,1,320,4096]{3,2,1,0:T(8,128)(2,1)}) %all-gather.3.cloned.1.call-update) | async-done | bytes 2621456 | tf_op jit(solution)/shard_map/all_gather | solution.py:45
  122.0 3.4 fusion.20
  129.4 14.3 %copy.56 = bf16[1,320,4096]{1,0,2:T(2,128)(2,1)} copy(bf16[1,320,4096]{2,1,0:T(8,128)(2,1)} %fusion.1) | data formatting | bytes 5242880 | tf_op jit(solution)/shard_map/convert_element_type | solution.py:78
  144.3 68.8 %reduce.16 = bf16[4096,320]{1,0:T(8,128)(2,1)} reduce(bf16[4096,1,320]{2,1,0:T(2,128)(2,1)} %bitcast.69, bf16[]{:T(256)} %broadcast.230), dimensions={1}, to_apply=%bitcast.55.reduce_sub_computation | reduce | bytes 5242882
  213.0 6.1 %reshape.387 = bf16[4,2,163840]{2,1,0:T(2,128)(2,1)} reshape(bf16[4096,320]{1,0:T(8,128)(2,1)} %reduce.16) | data formatting | bytes 5242880
  219.2 4.8 %all-to-all-start.3 = ((bf16[4,2,163840]{2,1,0:T(2,128)(2,1)}), bf16[4,2,163840]{2,1,0:T(2,128)(2,1)}, u32[]{:S(2)}, u32[]{:S(2)}) async-start(bf16[4,2,163840]{2,1,0:T(2,128)(2,1)} %reshape.387), calls=%async_computation.3 | async-start | bytes 5242880 | tf_op jit(solution)/shard_map/all_to_all | solution.py:79
  225.7 28.7 %collective-permute-done = f32[1,320]{1,0:T(1,128)S(1)} collective-permute-done((f32[1,320]{1,0:T(1,128)S(1)}, f32[1,320]{1,0:T(1,128)S(1)}, u32[]{:S(2)}, u32[]{:S(2)}) %collective-permute-start) | collective-permute-done | bytes 1312 | tf_op jit(solution)/shard_map/ppermute | solution.py:84
  258.9 4.6 %all-to-all-start.5 = ((f32[1,1,320]{1,0,2:T(1,128)}), f32[1,1,320]{1,0,2:T(1,128)S(1)}, u32[]{:S(2)}, u32[]{:S(2)}) async-start(f32[1,1,320]{1,0,2:T(1,128)} %copy.59), calls=%async_computation.5 | async-start | bytes 327680 | tf_op jit(solution)/shard_map/all_to_all | solution.py:87
  263.5 7.6 %reshape.388 = bf16[4096,1,320]{2,1,0:T(2,128)(2,1)} reshape(bf16[4,2,163840]{2,1,0:T(2,128)(2,1)} %all-to-all-done.3) | data formatting | bytes 5242880
  271.1 14.0 %copy.57 = bf16[1,320,4096]{2,1,0:T(8,128)(2,1)} copy(bf16[1,320,4096]{1,0,2:T(2,128)(2,1)} %bitcast.70) | data formatting | bytes 5242880 | tf_op jit(solution)/shard_map/all_to_all | solution.py:79
  285.0 7.3 %reshape.335 = f32[320,4,1024]{2,1,0:T(4,128)} reshape(bf16[1,320,4096]{2,1,0:T(8,128)(2,1)} %copy.57) | data formatting | bytes 7864320 | tf_op jit(solution)/shard_map/convert_element_type | solution.py:81
  292.4 5.7 %reduce_sum.54 = f32[320,1024]{1,0:T(8,128)S(1)} reduce(f32[320,4,1024]{2,1,0:T(4,128)} %reshape.335, f32[]{:T(128)} %constant.33.clone.1), dimensions={1}, to_apply=%region_5.6 | reduce | flops 983040 | bytes 6553604 | tf_op jit(solution)/shard_map/reduce_sum | solution.py:81
  300.1 5.1 %all-to-all-start.4 = ((f32[1,1,320,1024]{3,1,0,2:T(1,128)}), f32[1,1,320,1024]{3,1,0,2:T(1,128)S(1)}, u32[]{:S(2)}, u32[]{:S(2)}) async-start(f32[1,1,320,1024]{3,1,0,2:T(1,128)} %broadcast_in_dim.47), calls=%async_computation.4 | async-start | bytes 2621440 | tf_op jit(solution)/shard_map/all_to_all | solution.py:86
  305.5 4.3 %fusion.2 = bf16[1,256,4096]{2,1,0:T(8,128)(2,1)} fusion(bf16[320,256]{1,0:T(8,128)(2,1)S(1)} %get-tuple-element.40, bf16[1,1,320,4096]{3,2,1,0:T(8,128)(2,1)} %all-gather.5.cloned.1.call-done), kind=kOutput, calls=%fused_computation.11 | convolution fusion | flops 672137216 | bytes 4882432 | tf_op jit(solution)/shard_map/lrf,lrd->lfd/dot_general | solution.py:63
  309.8 4.5 %fusion.3 = bf16[1,256,4096]{2,1,0:T(8,128)(2,1)} fusion(bf16[320,256]{1,0:T(8,128)(2,1)S(1)} %get-tuple-element.41, bf16[1,1,320,4096]{3,2,1,0:T(8,128)(2,1)} %all-gather.5.cloned.1.call-done), kind=kOutput, calls=%fused_computation.12 | convolution fusion | flops 672137216 | bytes 4882432 | tf_op jit(solution)/shard_map/lrf,lrd->lfd/dot_general | solution.py:66
  314.3 2.7 fusion.4
  320.8 16.6 %all-to-all-done.4 = f32[1,1,320,1024]{3,1,0,2:T(1,128)S(1)} async-done(((f32[1,1,320,1024]{3,1,0,2:T(1,128)}), f32[1,1,320,1024]{3,1,0,2:T(1,128)S(1)}, u32[]{:S(2)}, u32[]{:S(2)}) %all-to-all-start.4) | async-done | bytes 1310752 | tf_op jit(solution)/shard_map/all_to_all | solution.py:86
  (80 shorter events, 34.5 us)
Async XLA Ops:
  8.0 72.6 %copy-start = (bf16[1,256,4096]{2,1,0:T(8,128)(2,1)S(1)}, bf16[1,256,4096]{2,1,0:T(8,128)(2,1)}, u32[]{:S(2)}) copy-start(bf16[1,256,4096]{2,1,0:T(8,128)(2,1)} %param.12) | copy-start | bytes 6291460
  8.0 2.6 copy-start.2
  8.0 72.6 %all-gather.5.cloned.1.call-start = ((), (), s32[]{:S(2)}) async-start(), calls=%async_computation.8 | async-start | bytes 3276800 | tf_op jit(solution)/shard_map/all_gather | solution.py:44
  10.6 2.7 copy-start.3
  17.5 45.9 %copy-start.8 = (bf16[128,1024]{1,0:T(8,128)(2,1)S(1)}, bf16[128,1024]{1,0:T(8,128)(2,1)}, u32[]{:S(2)}) copy-start(bf16[128,1024]{1,0:T(8,128)(2,1)} %param.15) | copy-start | bytes 786436
  42.0 80.0 %all-gather.3.cloned.1.call-start = ((), (), s32[]{:S(2)}) async-start(), calls=%async_computation.7 | async-start | bytes 3276800 | tf_op jit(solution)/shard_map/all_gather | solution.py:45
  63.3 280.3 %reduce-scatter.2.cloned.1.call-start = ((), (), s32[]{:S(2)}) async-start(), calls=%async_computation.9 | async-start | bytes 4718592 | tf_op jit(solution)/shard_map/reduce_scatter | solution.py:94
  66.2 0.7 copy-start.10
  80.6 2.8 copy-start.4
  80.6 3.2 copy-start.6
  125.4 1.6 copy-start.7
  219.2 39.7 %all-to-all-start.3 = ((bf16[4,2,163840]{2,1,0:T(2,128)(2,1)}), bf16[4,2,163840]{2,1,0:T(2,128)(2,1)}, u32[]{:S(2)}, u32[]{:S(2)}) async-start(bf16[4,2,163840]{2,1,0:T(2,128)(2,1)} %reshape.387), calls=%async_computation.3 | async-start | bytes 5242880 | tf_op jit(solution)/shard_map/all_to_all | solution.py:79
  224.0 30.4 %collective-permute-start = (f32[1,320]{1,0:T(1,128)S(1)}, f32[1,320]{1,0:T(1,128)S(1)}, u32[]{:S(2)}, u32[]{:S(2)}) collective-permute-start(f32[1,320]{1,0:T(1,128)S(1)} %reduce_sum.58), channel_id=1, source_target_pairs={{0,1},{1,0},{2,3},{3,2},{4,5},{5,4},{6,7},{7,6},{8,9},{9,8},{10,11... | collective-permute-start | bytes 3848 | tf_op jit(solution)/shard_map/ppermute | solution.py:84
  254.4 3.6 %collective-permute-start.1 = (f32[1,320]{1,0:T(1,128)S(1)}, f32[1,320]{1,0:T(1,128)S(1)}, u32[]{:S(2)}, u32[]{:S(2)}) collective-permute-start(f32[1,320]{1,0:T(1,128)S(1)} %reshape_add_fusion), channel_id=1, source_target_pairs={{0,2},{1,3},{2,0},{3,1},{4,6},{5,7},{6,4},{7,5},{8,10},{9,11},{10,... | collective-permute-start | bytes 3848 | tf_op jit(solution)/shard_map/ppermute | solution.py:84
  258.9 41.2 %all-to-all-start.5 = ((f32[1,1,320]{1,0,2:T(1,128)}), f32[1,1,320]{1,0,2:T(1,128)S(1)}, u32[]{:S(2)}, u32[]{:S(2)}) async-start(f32[1,1,320]{1,0,2:T(1,128)} %copy.59), calls=%async_computation.5 | async-start | bytes 327680 | tf_op jit(solution)/shard_map/all_to_all | solution.py:87
  298.1 7.1 %copy-start.9 = (s32[128,2]{0,1:T(2,128)S(1)}, s32[128,2]{0,1:T(2,128)}, u32[]{:S(2)}) copy-start(s32[128,2]{0,1:T(2,128)} %param.10) | copy-start | bytes 3076
  300.1 37.3 %all-to-all-start.4 = ((f32[1,1,320,1024]{3,1,0,2:T(1,128)}), f32[1,1,320,1024]{3,1,0,2:T(1,128)S(1)}, u32[]{:S(2)}, u32[]{:S(2)}) async-start(f32[1,1,320,1024]{3,1,0,2:T(1,128)} %broadcast_in_dim.47), calls=%async_computation.4 | async-start | bytes 2621440 | tf_op jit(solution)/shard_map/all_to_all | solution.py:86
  309.8 4.5 %copy-start.5 = (bf16[1,1,320,4096]{3,2,1,0:T(8,128)(2,1)S(1)}, bf16[1,1,320,4096]{3,2,1,0:T(8,128)(2,1)}, u32[]{:S(2)}) copy-start(bf16[1,1,320,4096]{3,2,1,0:T(8,128)(2,1)} %all-gather.3.cloned.1.call-done) | copy-start | bytes 7864324
  337.6 6.0 %copy-start.1 = (bf16[1,256,4096]{2,1,0:T(8,128)(2,1)S(1)}, bf16[1,256,4096]{2,1,0:T(8,128)(2,1)}, u32[]{:S(2)}) copy-start(bf16[1,256,4096]{2,1,0:T(8,128)(2,1)} %param.12) | copy-start | bytes 6291460
Sparse Core Ops, SparseCore 0:
  42.1 38.4 all-gather.4
  82.5 39.4 all-gather.2
Sparse Core Ops, SparseCore 1:
  66.7 48.8 reduce-scatter.1
